TPU v7x, 32 devices: a whole 2x2x4 slice. The times are simulated.
32 devices in a mesh: ep: 16 (over z, y, x), tp: 2 (over core).
Axes of the slice: x: 2, y: 2, z: 4, core: 2. Of those that a mesh axis runs over, the one named last changes fastest.
Arguments:
- tokens: bfloat16 [8192, 2048], P(('ep', 'tp')), may hold values from -6 to 6
- norm_gain: float32 [2048], replicated, may hold values from 0.1 to 1.9
- norm_bias: float32 [2048], replicated, may hold values from -3 to 3
- gate_weight: bfloat16 [16, 2048, 1024], P('ep', None, 'tp'), may hold values from -0.125 to 0.125
- up_weight: bfloat16 [16, 2048, 1024], P('ep', None, 'tp'), may hold values from -0.125 to 0.125
- down_weight: bfloat16 [16, 1024, 2048], P('ep', 'tp'), may hold values from -0.1875 to 0.1875
- expert_ids: int32 [8192, 2], P(('ep', 'tp')), may hold values from 0 to 15, all different within a row; in each aligned block of 256 rows (0 to 255, 256 to 511, ...) at most 64 rows name the same one
- route_weights: float32 [8192, 2], P(('ep', 'tp')), may hold values from 0.2 to 1
Outputs:
- mixed: bfloat16 [8192, 2048], P(('ep', 'tp'))
Inputs may be any that keep to these rules, and one draw needn't show every extreme that they name: `expert_ids`: a token's 2 experts differ; in the tokens of one device (aligned blocks of 256 rows) no expert is named by more than 64 entries, a bound that some block reaches.
All inputs are finite; a program needn't handle non-finite values.
Results may differ from a plain program's by a relative error of at most 0.0071.
Values may be sent and summed in bfloat16 or wider, within the bound.
A program may use at most 128 MiB of HBM per device.

v0:
```python
import functools

import jax
import jax.numpy as jnp
from jax import lax
from jax.experimental import pallas as pl
from jax.experimental.pallas import tpu as pltpu
from jax.sharding import PartitionSpec as P

MESH = pl.DeviceIdType.MESH
LINE = 4
CHUNKS = 8
LAG = 2


def kernel(
    planes, raw, gain, bias, meta, gw, uw, dw, out,
    src, tok, met, wg, wu, wd, sel, mix, snd, xin, hid, res, ret, psend, racc,
    s_own, s_met, s_mets, s_wl, s_ws, s_wr, s_tok, s_toks, s_x, s_xs, s_r, s_rs, s_p, s_ps,
):
    n = LINE
    side = planes
    me, core = lax.axis_index("ep"), lax.axis_index("tp")
    z, p = me // side, lax.rem(me, side)
    tokens, width = raw.shape
    half = gw.shape[2]
    rows = snd.shape[1]
    cap = rows // side
    k = CHUNKS
    wide = width // k
    end = (z == 0) | (z == n - 1)
    mid = jnp.logical_not(end)
    step = jnp.where(z < n // 2, 1, -1)
    za, zb = z + step, z - step
    order = [
        z,
        jnp.where(end, z + 3 * step, z + 2 * step),
        jnp.where(end, z + 2 * step, z - step),
        z + step,
    ]

    def cols(c):
        return pl.ds(pl.multiple_of(c * wide, wide), wide)

    def band(i):
        return pl.ds(pl.multiple_of(i * cap, cap), cap)

    def plane(t):
        return {"ep": t * side + p}

    def peer(j):
        return lax.rem(p + j, side)

    def remote(src, dst, send, recv, where):
        return pltpu.make_async_remote_copy(
            src_ref=src, dst_ref=dst, send_sem=send, recv_sem=recv,
            device_id=where, device_id_type=MESH,
        )

    def landed(ref, sem):
        pltpu.make_async_copy(ref, ref, sem).wait()

    barrier = pltpu.get_barrier_semaphore()
    own = pltpu.make_async_copy(raw, src, s_own.at[0])
    own.start()
    ownm = pltpu.make_async_copy(meta, met.at[z], s_own.at[1])
    ownm.start()
    for j in range(1, side):
        pl.semaphore_signal(
            barrier, inc=1, device_id={"ep": z * side + peer(j)}, device_id_type=MESH
        )
    for j in range(1, n):
        pl.semaphore_signal(
            barrier, inc=1, device_id=plane(lax.rem(z + j, n)), device_id_type=MESH
        )
    pl.semaphore_signal(barrier, inc=1, device_id={"tp": 1 - core}, device_id_type=MESH)

    def send_tok(s, c, to, way):
        remote(
            tok.at[s, :, cols(c)], tok.at[s, :, cols(c)],
            s_toks.at[way, s], s_tok.at[s, c], plane(to),
        ).start()

    def send_own(to, way):
        @pl.loop(0, k)
        def _(c):
            send_tok(z, c, to, way)

    def prep(q):
        s = order[q]
        ids0, ids1 = met[s, 0:1, :], met[s, 1:2, :]
        wt0, wt1 = met[s, 2:3, :], met[s, 3:4, :]
        row = lax.broadcasted_iota(jnp.int32, (rows, tokens), 0)
        e_row = (z * side + row // cap).astype(jnp.float32)
        s_row = lax.rem(row, cap).astype(jnp.float32)
        hit0 = (ids0 == e_row).astype(jnp.float32)
        hit1 = (ids1 == e_row).astype(jnp.float32)
        hit = hit0 + hit1
        before = (
            lax.broadcasted_iota(jnp.int32, (tokens, tokens), 0)
            < lax.broadcasted_iota(jnp.int32, (tokens, tokens), 1)
        ).astype(jnp.float32).astype(jnp.bfloat16)
        count = jnp.dot(hit.astype(jnp.bfloat16), before, preferred_element_type=jnp.float32)
        pick = jnp.where(count == s_row, hit, 0.0)
        sel[q] = pick.astype(jnp.bfloat16)
        w = pick * (hit0 * wt0 + hit1 * wt1)
        high = w.astype(jnp.bfloat16)
        mix[q, 0] = high
        mix[q, 1] = (w - high.astype(jnp.float32)).astype(jnp.bfloat16)

    own.wait()
    slab = min(32, tokens)

    @pl.loop(0, tokens // slab)
    def _(i):
        at = pl.ds(pl.multiple_of(i * slab, slab), slab)
        v = src[at, :].astype(jnp.float32)
        v = v - jnp.mean(v, axis=-1, keepdims=True)
        spread = jnp.mean(v * v, axis=-1, keepdims=True)
        y = v * lax.rsqrt(spread + 1e-05) * gain[...] + bias[...]
        tok[z, at, :] = y.astype(jnp.bfloat16)

    ownm.wait()
    prep(0)
    pl.semaphore_wait(barrier, side - 1 + n)
    for j in range(1, n):
        remote(
            met.at[z], met.at[z], s_mets.at[j - 1], s_met.at[z], plane(lax.rem(z + j, n))
        ).start()

    @pl.when(end)
    def _():
        send_own(za, 0)

    halfrows = pl.ds(pl.multiple_of(core * half, half), half)
    pairs = [
        (gw.at[0], wg.at[core]), (uw.at[0], wu.at[core]), (dw.at[0], wd.at[halfrows]),
    ]
    for i, (a, b) in enumerate(pairs):
        pltpu.make_async_copy(a, b, s_wl.at[i]).start()
        remote(a, b, s_ws.at[i], s_wr.at[i], {"tp": 1 - core}).start()

    def disp(q, c):
        y = jnp.dot(sel[q], tok[order[q], :, cols(c)], preferred_element_type=jnp.float32)
        snd[q, :, cols(c)] = y.astype(jnp.bfloat16)
        xin[q, band(p), cols(c)] = snd[q, band(p), cols(c)]
        for j in range(1, side):
            o = peer(j)
            remote(
                snd.at[q, band(o), cols(c)], xin.at[q, band(p), cols(c)],
                s_xs.at[q], s_x.at[q], {"ep": z * side + o},
            ).start()

    def others(ref, q):
        return ref.at[q, pl.ds(0, (side - 1) * cap)]

    tile = min(256, half)
    per = half // tile

    def gate(q, i):
        h, at = i // per, lax.rem(i, per)
        part = pl.ds(pl.multiple_of(at * tile, tile), tile)
        x = xin[q]
        g = jnp.dot(x, wg[h, :, part], preferred_element_type=jnp.float32)
        u = jnp.dot(x, wu[h, :, part], preferred_element_type=jnp.float32)
        v = g / (1.0 + jnp.exp(-g)) * u
        hid[:, pl.ds(pl.multiple_of(i * tile, tile), tile)] = v.astype(jnp.bfloat16)

    def down(q):
        @pl.loop(0, k)
        def _(c):
            y = jnp.dot(hid[...], wd[:, cols(c)], preferred_element_type=jnp.float32)
            res[q, :, cols(c)] = y.astype(jnp.bfloat16)
            ret[q, band(p), cols(c)] = res[q, band(p), cols(c)]
            for j in range(1, side):
                o = peer(j)
                remote(
                    res.at[q, band(o), cols(c)], ret.at[q, band(p), cols(c)],
                    s_rs.at[q], s_r.at[q, c], {"ep": z * side + o},
                ).start()

    def compute(q):
        landed(others(xin, q), s_x.at[q])
        pl.loop(0, 2 * per)(lambda i: gate(q, i))
        down(q)

    def weigh(q, c):
        landed(ret.at[q, pl.ds(0, (side - 1) * cap), cols(c)], s_r.at[q, c])
        r = ret[q, :, cols(c)]
        dims = (((0,), (0,)), ((), ()))
        return lax.dot_general(
            mix[q, 0], r, dims, preferred_element_type=jnp.float32
        ) + lax.dot_general(mix[q, 1], r, dims, preferred_element_type=jnp.float32)

    def combine(q, c, add):
        t = order[q]
        y = weigh(q, c)
        to = zb if (q == 2 and add) else za
        if add:
            landed(racc.at[t, c], s_p.at[t, c])
            y = y + racc[t, c].astype(jnp.float32)
        psend[q - 1, c] = y.astype(jnp.bfloat16)
        slot = jnp.where((to == t) & (to < z), n, t)
        remote(
            psend.at[q - 1, c], racc.at[slot, c], s_ps.at[q - 1], s_p.at[slot, c], plane(to)
        ).start()

    def arrived(s, c):
        landed(tok.at[s, :, cols(c)], s_tok.at[s, c])

    @pl.loop(0, k)
    def _(c):
        disp(0, c)

    for q in range(1, n):
        landed(met.at[order[q]], s_met.at[order[q]])
        prep(q)

    def near(c):
        arrived(order[2], c)
        send_tok(order[2], c, za, 0)
        disp(2, c)

    def far(c):
        arrived(order[1], c)
        send_tok(order[1], c, zb, 1)
        disp(1, c)

    def weights():
        for i, (a, b) in enumerate(pairs):
            pltpu.make_async_copy(a, b, s_wl.at[i]).wait()
            landed(b, s_wr.at[i])

    @pl.when(mid)
    def _():
        def pass_on(c):
            arrived(order[3], c)
            send_tok(order[3], c, zb, 1)
            disp(3, c)

        for c in range(LAG):
            near(c)

        @pl.loop(LAG, k)
        def _(c):
            near(c)
            far(c - LAG)

        send_own(za, 0)
        pl.loop(k - LAG, k)(far)
        weights()
        pl.loop(0, k // 2)(pass_on)
        landed(others(xin, 1), s_x.at[1])
        turns = k - k // 2
        for j in range(turns):
            pass_on(k // 2 + j)
            for i in range(j * 2 * per // turns, (j + 1) * 2 * per // turns):
                gate(1, i)
        send_own(zb, 1)
        down(1)
        compute(2)
        compute(3)
        for c in range(LAG):
            combine(1, c, True)

        @pl.loop(LAG, k)
        def _(c):
            combine(1, c, True)
            combine(2, c - LAG, True)

        pl.loop(k - LAG, k)(lambda c: combine(2, c, True))
        compute(0)
        pl.loop(0, k)(lambda c: combine(3, c, True))

    @pl.when(end)
    def _():
        def take(c):
            arrived(order[1], c)
            disp(1, c)

        pl.loop(0, k // 2)(take)
        weights()
        compute(0)
        pl.loop(k // 2, k)(take)
        compute(1)

        @pl.loop(0, k)
        def _(c):
            arrived(order[2], c)
            disp(2, c)
            combine(1, c, False)

        compute(2)

        @pl.loop(0, k)
        def _(c):
            combine(2, c, False)
            arrived(order[3], c)
            disp(3, c)

        compute(3)
        pl.loop(0, k)(lambda c: combine(3, c, False))

    def last(c, slots):
        y = weigh(0, c)
        for slot in slots:
            landed(racc.at[slot, c], s_p.at[slot, c])
            y = y + racc[slot, c].astype(jnp.float32)
        out[:, cols(c)] = y.astype(out.dtype)

    @pl.when(end)
    def _():
        pl.loop(0, k)(lambda c: last(c, [jnp.where(z == 0, n, z)]))

    @pl.when(mid)
    def _():
        pl.loop(0, k)(lambda c: last(c, [z, n]))

    drain = landed

    for j in range(1, n):
        drain(met.at[z], s_mets.at[j - 1])
    for i, (a, b) in enumerate(pairs):
        drain(b, s_ws.at[i])
    drain(tok.at[z], s_toks.at[0, z])

    @pl.when(mid)
    def _():
        drain(tok.at[z], s_toks.at[1, z])
        drain(tok.at[z], s_toks.at[0, order[2]])
        drain(tok.at[z], s_toks.at[1, order[1]])
        drain(tok.at[z], s_toks.at[1, order[3]])

    for q in range(n):
        drain(others(snd, q), s_xs.at[q])
        drain(others(res, q), s_rs.at[q])
    for q in range(1, n):
        drain(psend.at[q - 1], s_ps.at[q - 1])


def body(
    tokens, norm_gain, norm_bias, gate_weight, up_weight, down_weight, expert_ids, route_weights
):
    count, width = tokens.shape
    experts = lax.axis_size("ep")
    cap = max(4 * count // experts, 4)
    side = experts // LINE
    half = gate_weight.shape[2]
    both = jnp.concatenate([expert_ids.astype(jnp.float32), route_weights], axis=1)
    meta = jnp.pad(both.T, ((0, 4), (0, 0)))
    rows = side * cap
    wide = width // CHUNKS
    bf = jnp.bfloat16
    dma = pltpu.SemaphoreType.DMA
    vmem = pl.BlockSpec(memory_space=pltpu.VMEM)
    hbm = pl.BlockSpec(memory_space=pl.ANY)
    return pl.pallas_call(
        functools.partial(kernel, side),
        out_shape=jax.ShapeDtypeStruct((count, width), bf),
        in_specs=[hbm, vmem, vmem] + [hbm] * 4,
        out_specs=pl.BlockSpec(memory_space=pltpu.VMEM),
        scratch_shapes=[
            pltpu.VMEM((count, width), bf),
            pltpu.VMEM((LINE, count, width), bf),
            pltpu.VMEM((LINE, 8, count), jnp.float32),
            pltpu.VMEM((2, width, half), bf),
            pltpu.VMEM((2, width, half), bf),
            pltpu.VMEM((2 * half, width), bf),
            pltpu.VMEM((LINE, rows, count), bf),
            pltpu.VMEM((LINE, 2, rows, count), bf),
            pltpu.VMEM((LINE, rows, width), bf),
            pltpu.VMEM((LINE, rows, width), bf),
            pltpu.VMEM((rows, 2 * half), bf),
            pltpu.VMEM((LINE, rows, width), bf),
            pltpu.VMEM((LINE, rows, width), bf),
            pltpu.VMEM((LINE - 1, CHUNKS, count, wide), bf),
            pltpu.VMEM((LINE + 1, CHUNKS, count, wide), bf),
            dma((2,)),
            dma((LINE,)),
            dma((LINE - 1,)),
            dma((3,)),
            dma((3,)),
            dma((3,)),
            dma((LINE, CHUNKS)),
            dma((2, LINE)),
            dma((LINE,)),
            dma((LINE,)),
            dma((LINE, CHUNKS)),
            dma((LINE,)),
            dma((LINE + 1, CHUNKS)),
            dma((LINE - 1,)),
        ],
        compiler_params=pltpu.CompilerParams(
            collective_id=0, has_side_effects=True, vmem_limit_bytes=60 * 1024 * 1024
        ),
    )(tokens, norm_gain[None], norm_bias[None], meta, gate_weight, up_weight, down_weight)


def solution(mesh):
    placed = (
        P(("ep", "tp"), None),
        P(),
        P(),
        P("ep", None, "tp"),
        P("ep", None, "tp"),
        P("ep", "tp", None),
        P(("ep", "tp"), None),
        P(("ep", "tp"), None),
    )
    return jax.shard_map(
        body, mesh=mesh, in_specs=placed, out_specs=P(("ep", "tp"), None), check_vma=False
    )
```

profile of v0, /device:TPU:0, one launch (start us, length us, event | category | flops | bytes accessed | tf_op | source)
XLA Modules:
  0.0 134.0 jit_solution(4084023963667462290)
XLA Ops:
  0.0 0.7 convert_element_type.5
  0.7 0.7 maximum_bitcast_fusion
  1.4 0.6 pad.4.meta
  2.0 129.7 %shard_map.82 = bf16[256,2048]{1,0:T(8,128)(2,1)} custom-call(bf16[256,2048]{1,0:T(8,128)(2,1)} %raw.1, f32[1,2048]{1,0:T(1,128)} %bitcast.4, f32[1,2048]{1,0:T(1,128)} %bitcast.5, f32[8,256]{1,0:T(8,128)} %pad.4.meta, bf16[1,2048,512]{2,1,0:T(8,128)(2,1)} %gw.1, bf16[1,2048,512]{2,1,0:T(8,128)(2,1)} %uw.1, bf16[1,512,2048]{2,1,0:T(8,128)(2,1)} %dw.1), custom_call_target="tpu_custom_call" | custom-call | tf_op jit(solution)/shard_map/pallas_call | solution.py:357
  131.7 2.3 %copy.10 = bf16[256,2048]{1,0:T(8,128)(2,1)} copy(bf16[256,2048]{1,0:T(8,128)(2,1)} %shard_map.82) | data formatting | bytes 2097152
where the time goes:
time: 135 us; the launch traced here: 134 us
  Pallas kernels  130 us (96%)
  local copies, waits for them, and re-layouts  2.91 us (2%)
  other arithmetic  1.37 us (1%)
    pallas_call x1, Pallas kernels, body(): pl.pallas_call(functools.partial(kernel, side), out_shape=jax.ShapeDtypeS...  130 us

commit v1 on v0

v1 whole, which is shorter than its diff:
```python
import functools

import jax
import jax.numpy as jnp
from jax import lax
from jax.experimental import pallas as pl
from jax.experimental.pallas import tpu as pltpu
from jax.sharding import PartitionSpec as P

MESH = pl.DeviceIdType.MESH
LINE = 4
CHUNKS = 4


def kernel(
    planes, raw, gain, bias, ids, rw, gw, uw, dw, out,
    src, oth, tok, met, wg, wu, wd, sel, mix, snd, xin, hid, res, ret, psend, racc, obuf,
    s_own, s_wl, s_ws, s_wr, s_tok, s_toks, s_met, s_mets, s_os, s_x, s_xs, s_xd, s_xds,
    s_h, s_hs, s_r, s_rs, s_p, s_ps, s_ol, s_or, s_od,
):
    n = LINE
    side = planes
    me, core = lax.axis_index("ep"), lax.axis_index("tp")
    other = 1 - core
    z, p = me // side, lax.rem(me, side)
    tokens, width = raw.shape
    half = gw.shape[2]
    span = width // 2
    rows = snd.shape[2]
    cap = rows // side
    k = CHUNKS
    wide = span // k
    end = (z == 0) | (z == n - 1)
    mid = jnp.logical_not(end)
    step = jnp.where(z < n // 2, 1, -1)
    za, zb = z + step, z - step
    order = [
        z,
        jnp.where(end, z + 3 * step, z + 2 * step),
        jnp.where(end, z + 2 * step, z - step),
        z + step,
    ]

    def cols(c):
        return pl.ds(pl.multiple_of(c * wide, wide), wide)

    def part(h, size):
        return pl.ds(pl.multiple_of(h * size, size), size)

    def band(i):
        return pl.ds(pl.multiple_of(i * cap, cap), cap)

    def plane(t):
        return {"ep": t * side + p}

    partner = {"tp": other}

    def peer(j):
        return lax.rem(p + j, side)

    def remote(src, dst, send, recv, where):
        pltpu.make_async_remote_copy(
            src_ref=src, dst_ref=dst, send_sem=send, recv_sem=recv,
            device_id=where, device_id_type=MESH,
        ).start()

    def landed(ref, sem):
        pltpu.make_async_copy(ref, ref, sem).wait()

    barrier = pltpu.get_barrier_semaphore()
    own = pltpu.make_async_copy(raw, src, s_own)
    own.start()

    def greet(where):
        pl.semaphore_signal(barrier, inc=1, device_id=where, device_id_type=MESH)

    greet(partner)
    greet(plane(za))

    @pl.when(mid)
    def _():
        greet(plane(zb))

    for j in range(1, side):
        greet({"ep": z * side + peer(j)})

    mine = part(core, half)
    loads = [
        (gw.at[0], wg), (uw.at[0], wu), (dw.at[0, :, part(core, span)], wd.at[mine]),
    ]
    for i, (a, b) in enumerate(loads):
        pltpu.make_async_copy(a, b, s_wl.at[i]).start()

    met[z, core, 0:2, :] = ids[...].astype(jnp.float32)
    met[z, core, 2:4, :] = rw[...]

    own.wait()
    slab = min(32, tokens)

    @pl.loop(0, tokens // slab)
    def _(i):
        at = pl.ds(pl.multiple_of(i * slab, slab), slab)
        v = src[at, :].astype(jnp.float32)
        v = v - jnp.mean(v, axis=-1, keepdims=True)
        spread = jnp.mean(v * v, axis=-1, keepdims=True)
        y = v * lax.rsqrt(spread + 1e-05) * gain[...] + bias[...]
        y = y.astype(jnp.bfloat16)
        lo, hi = y[:, :span], y[:, span:]
        tok[z, core, at, :] = jnp.where(core == 0, lo, hi)
        oth[at, :] = jnp.where(core == 0, hi, lo)

    pl.semaphore_wait(barrier, side + 1 + jnp.where(mid, 1, 0))

    remote(met.at[z, core], met.at[z, core], s_os.at[0], s_met.at[z, core], partner)
    for c in range(k):
        remote(
            oth.at[:, cols(c)], tok.at[z, core, :, cols(c)], s_os.at[1], s_tok.at[z, core, c], partner
        )
    remote(
        dw.at[0, :, part(other, span)], wd.at[mine], s_ws, s_wr, partner
    )

    def send_tok(s, b, c, to, way):
        at = tok.at[s, b, :, cols(c)]
        remote(at, at, s_toks.at[way, s, b], s_tok.at[s, b, c], plane(to))

    def send_met(s, b, to, way):
        at = met.at[s, b]
        remote(at, at, s_mets.at[way, s, b], s_met.at[s, b], plane(to))

    def arrived(s, b, c):
        landed(tok.at[s, b, :, cols(c)], s_tok.at[s, b, c])

    def got_met(s, b):
        landed(met.at[s, b], s_met.at[s, b])

    def own_tok(b):
        for c in range(k):
            @pl.when(core != b)
            def _():
                arrived(z, b, c)

            send_tok(z, b, c, za, 0)

    def own_tok_b(b):
        for c in range(k):
            send_tok(z, b, c, zb, 1)

    def prep(q, b, s=None):
        s = order[q] if s is None else s
        ids0, ids1 = met[s, b, 0:1, :], met[s, b, 1:2, :]
        wt0, wt1 = met[s, b, 2:3, :], met[s, b, 3:4, :]
        row = lax.broadcasted_iota(jnp.int32, (rows, tokens), 0)
        e_row = (z * side + row // cap).astype(jnp.float32)
        s_row = lax.rem(row, cap).astype(jnp.float32)
        hit0 = (ids0 == e_row).astype(jnp.float32)
        hit1 = (ids1 == e_row).astype(jnp.float32)
        hit = hit0 + hit1
        before = (
            lax.broadcasted_iota(jnp.int32, (tokens, tokens), 0)
            < lax.broadcasted_iota(jnp.int32, (tokens, tokens), 1)
        ).astype(jnp.float32).astype(jnp.bfloat16)
        count = jnp.dot(hit.astype(jnp.bfloat16), before, preferred_element_type=jnp.float32)
        pick = jnp.where(count == s_row, hit, 0.0)
        sel[q, b] = pick.astype(jnp.bfloat16)
        w = (pick * (hit0 * wt0 + hit1 * wt1)).T
        high = w.astype(jnp.bfloat16)
        mix[q, b, 0] = high
        mix[q, b, 1] = (w - high.astype(jnp.float32)).astype(jnp.bfloat16)

    def disp(q, b, c, s=None):
        s = order[q] if s is None else s
        y = jnp.dot(sel[q, b], tok[s, b, :, cols(c)], preferred_element_type=jnp.float32)
        snd[q, b, :, cols(c)] = y.astype(jnp.bfloat16)
        xin[q, b, core, band(p), cols(c)] = snd[q, b, band(p), cols(c)]
        for j in range(1, side):
            o = peer(j)
            remote(
                snd.at[q, b, band(o), cols(c)], xin.at[q, b, core, band(p), cols(c)],
                s_xs.at[q, b], s_x.at[q, b], {"ep": z * side + o},
            )

    def others(ref):
        return ref.at[pl.ds(0, (side - 1) * cap)]

    def swap_x(q, b):
        landed(others(xin.at[q, b, core]), s_x.at[q, b])
        at = xin.at[q, b, core]
        remote(at, at, s_xds.at[q, b], s_xd.at[q, b], partner)

    tile = min(256, half)

    def gate(q, b):
        landed(xin.at[q, b, other], s_xd.at[q, b])

        @pl.loop(0, half // tile)
        def _(i):
            at = part(i, tile)
            lo, hi = xin[q, b, 0], xin[q, b, 1]
            g = jnp.dot(lo, wg[:span, at], preferred_element_type=jnp.float32)
            g = g + jnp.dot(hi, wg[span:, at], preferred_element_type=jnp.float32)
            u = jnp.dot(lo, wu[:span, at], preferred_element_type=jnp.float32)
            u = u + jnp.dot(hi, wu[span:, at], preferred_element_type=jnp.float32)
            v = g / (1.0 + jnp.exp(-g)) * u
            hid[q, b, core, :, at] = v.astype(jnp.bfloat16)

        at = hid.at[q, b, core]
        remote(at, at, s_hs.at[q, b], s_h.at[q, b], partner)

    def down(q, b, c):
        @pl.when(c == 0)
        def _():
            landed(hid.at[q, b, other], s_h.at[q, b])

        y = jnp.dot(hid[q, b, 0], wd[:half, cols(c)], preferred_element_type=jnp.float32)
        y = y + jnp.dot(hid[q, b, 1], wd[half:, cols(c)], preferred_element_type=jnp.float32)
        res[q, b, :, cols(c)] = y.astype(jnp.bfloat16)
        ret[q, b, band(p), cols(c)] = res[q, b, band(p), cols(c)]
        for j in range(1, side):
            o = peer(j)
            remote(
                res.at[q, b, band(o), cols(c)], ret.at[q, b, band(p), cols(c)],
                s_rs.at[q, b], s_r.at[q, b, c], {"ep": z * side + o},
            )

    def downs(q, b):
        pl.loop(0, k)(lambda c: down(q, b, c))

    def weigh(q, b, c):
        landed(others(ret.at[q, b, :, cols(c)]), s_r.at[q, b, c])
        r = ret[q, b, :, cols(c)]
        return jnp.dot(mix[q, b, 0], r, preferred_element_type=jnp.float32) + jnp.dot(
            mix[q, b, 1], r, preferred_element_type=jnp.float32
        )

    def combine(q, b, c, t, to, add):
        y = weigh(q, b, c)
        if add:
            landed(racc.at[t, b, c], s_p.at[t, b, c])
            y = y + racc[t, b, c].astype(jnp.float32)
        psend[q - 1, b, c] = y.astype(jnp.bfloat16)
        slot = jnp.where((to == t) & (to < z), n, t)
        remote(
            psend.at[q - 1, b, c], racc.at[slot, b, c], s_ps.at[q - 1, b], s_p.at[slot, b, c], plane(to)
        )

    def weights():
        for i, (a, b) in enumerate(loads):
            pltpu.make_async_copy(a, b, s_wl.at[i]).wait()
        landed(wd.at[part(other, half)], s_wr)

    def own_met(b):
        send_met(z, b, za, 0)

        @pl.when(mid)
        def _():
            send_met(z, b, zb, 1)

    own_met(core)
    own_tok(0)

    @pl.when(mid)
    def _():
        own_tok_b(0)

    got_met(z, other)
    own_met(other)
    prep(0, 0)
    pl.loop(0, k)(lambda c: disp(0, 0, c))

    @pl.when(end)
    def _():
        own_tok(1)

    @pl.when(mid)
    def _():
        @pl.when(core != 1)
        def _():
            for c in range(k):
                arrived(z, 1, c)

    prep(0, 1)

    @pl.when(mid)
    def _():
        def relay(q, b, c):
            s = order[q]
            arrived(s, b, c)
            send_tok(s, b, c, za if q == 2 else zb, 0 if q == 2 else 1)

        def learn(q, b):
            got_met(order[q], b)
            send_met(order[q], b, za if q == 2 else zb, 0 if q == 2 else 1)
            prep(q, b)

        def fold(q, b, c):
            combine(q, b, c, order[q], zb if q == 2 else za, True)

        def folds(q, b, lo, hi):
            pl.loop(lo, hi)(lambda c: fold(q, b, c))

        learn(3, 0)
        learn(2, 0)

        @pl.loop(0, k)
        def _(c):
            relay(3, 0, c)
            relay(2, 0, c)
            disp(3, 0, c)
            disp(0, 1, c)

        learn(1, 0)
        learn(2, 1)

        @pl.loop(0, k)
        def _(c):
            relay(1, 0, c)
            relay(2, 1, c)
            disp(1, 0, c)
            disp(2, 0, c)

            @pl.when(c == 0)
            def _():
                weights()
                swap_x(0, 0)

            @pl.when(c == 1)
            def _():
                swap_x(3, 0)
                gate(0, 0)

            @pl.when(c == 2)
            def _():
                gate(3, 0)

        pl.loop(0, k)(lambda c: send_tok(z, 1, c, za, 0))
        learn(1, 1)

        @pl.loop(0, k)
        def _(c):
            relay(1, 1, c)
            disp(1, 1, c)
            down(3, 0, c)

            @pl.when(c == 1)
            def _():
                swap_x(0, 1)
                swap_x(1, 0)

            @pl.when(c == 2)
            def _():
                gate(1, 0)

        learn(3, 1)
        gate(0, 1)

        @pl.loop(0, k)
        def _(c):
            relay(3, 1, c)
            disp(3, 1, c)
            down(1, 0, c)

            @pl.when(c == 0)
            def _():
                swap_x(2, 0)

            @pl.when(c == 1)
            def _():
                swap_x(1, 1)
                gate(2, 0)

            @pl.when(c == 2)
            def _():
                gate(1, 1)

            @pl.when(c > 0)
            def _():
                fold(3, 0, c - 1)

        pl.loop(0, k)(lambda c: send_tok(z, 1, c, zb, 1))
        pl.loop(0, k)(lambda c: disp(2, 1, c))
        fold(3, 0, k - 1)
        downs(1, 1)
        folds(1, 0, 0, k // 2)
        swap_x(3, 1)
        downs(2, 0)
        folds(1, 0, k // 2, k)
        swap_x(2, 1)
        gate(3, 1)
        downs(3, 1)
        gate(2, 1)

        @pl.loop(0, k // 2)
        def _(c):
            fold(1, 1, c)
            fold(2, 0, c)

        downs(2, 1)

        @pl.loop(k // 2, k)
        def _(c):
            fold(1, 1, c)
            fold(2, 0, c)

        downs(0, 0)

        @pl.loop(0, k // 2)
        def _(c):
            fold(3, 1, c)
            fold(2, 1, c)

        downs(0, 1)

        @pl.loop(k // 2, k)
        def _(c):
            fold(3, 1, c)
            fold(2, 1, c)

    @pl.when(end)
    def _():
        pl.loop(0, k)(lambda c: disp(0, 1, c))

        def take(q, b, c):
            s = z + (n - q) * step
            arrived(s, b, c)
            disp(q, b, c, s)

        def learn(q, b):
            s = z + (n - q) * step
            got_met(s, b)
            prep(q, b, s)

        def unit(i):
            return jnp.where(i < 3, 3 - i, i - 2), jnp.where(i < 3, 0, 1)

        def fold(q, b, c):
            combine(q, b, c, z + (n - q) * step, za, False)

        learn(3, 0)

        @pl.loop(0, k)
        def _(c):
            take(3, 0, c)

            @pl.when(c == 1)
            def _():
                weights()
                swap_x(0, 0)

            @pl.when(c == 2)
            def _():
                gate(0, 0)

        quarter = k // 4

        @pl.loop(0, 5)
        def _(i):
            q, b = unit(i)
            q1, b1 = unit(i + 1)
            q0, b0 = unit(jnp.maximum(i - 1, 0))

            def more(j):
                pl.loop(j * quarter, (j + 1) * quarter)(lambda c: take(q1, b1, c))

            def back(j):
                pl.when(i > 0)(lambda: pl.loop(j * quarter, (j + 1) * quarter)(lambda c: fold(q0, b0, c)))

            learn(q1, b1)
            more(0)
            swap_x(q, b)
            back(1)
            more(1)
            gate(q, b)
            back(2)
            more(2)
            pl.loop(0, k // 2)(lambda c: down(q, b, c))
            back(3)
            more(3)
            pl.loop(k // 2, k)(lambda c: down(q, b, c))
            pl.loop(0, quarter)(lambda c: fold(q, b, c))

            @pl.when(i == 0)
            def _():
                swap_x(0, 1)
                downs(0, 0)
                gate(0, 1)

        swap_x(3, 1)
        pl.loop(quarter, 2 * quarter)(lambda c: fold(2, 1, c))
        gate(3, 1)
        pl.loop(2 * quarter, k)(lambda c: fold(2, 1, c))
        downs(3, 1)
        downs(0, 1)
        pl.loop(0, k)(lambda c: fold(3, 1, c))

    def last(b, c, slots):
        y = weigh(0, b, c)
        for slot in slots:
            landed(racc.at[slot, b, c], s_p.at[slot, b, c])
            y = y + racc[slot, b, c].astype(jnp.float32)
        obuf[b, c] = y.astype(out.dtype)
        to = out.at[:, pl.ds(pl.multiple_of(core * span + c * wide, wide), wide)]

        @pl.when(core == b)
        def _():
            pltpu.make_async_copy(obuf.at[b, c], to, s_ol).start()

        @pl.when(core != b)
        def _():
            remote(obuf.at[b, c], to, s_od, s_or, partner)

    @pl.when(end)
    def _():
        for b in range(2):
            pl.loop(0, k)(lambda c: last(b, c, [jnp.where(z == 0, n, z)]))

    @pl.when(mid)
    def _():
        for b in range(2):
            pl.loop(0, k)(lambda c: last(b, c, [z, n]))

    drain = landed
    drain(met.at[z, core], s_os.at[0])
    drain(oth, s_os.at[1])
    drain(wd.at[mine], s_ws)
    for b in range(2):
        drain(tok.at[z, b], s_toks.at[0, z, b])
        drain(met.at[z, b], s_mets.at[0, z, b])

    @pl.when(mid)
    def _():
        for b in range(2):
            for way, s in ((1, z), (0, order[2]), (1, order[1]), (1, order[3])):
                drain(tok.at[s, b], s_toks.at[way, s, b])
                drain(met.at[s, b], s_mets.at[way, s, b])

    for q in range(n):
        for b in range(2):
            drain(others(snd.at[q, b]), s_xs.at[q, b])
            drain(others(res.at[q, b]), s_rs.at[q, b])
            drain(xin.at[q, b, core], s_xds.at[q, b])
            drain(hid.at[q, b, core], s_hs.at[q, b])
            if q > 0:
                drain(psend.at[q - 1, b], s_ps.at[q - 1, b])
    drain(obuf.at[0], s_ol)
    drain(obuf.at[0], s_od)
    drain(obuf.at[0], s_or)


def body(
    tokens, norm_gain, norm_bias, gate_weight, up_weight, down_weight, expert_ids, route_weights
):
    count, width = tokens.shape
    experts = lax.axis_size("ep")
    cap = max(4 * count // experts, 4)
    side = experts // LINE
    half = gate_weight.shape[2]
    rows = side * cap
    span = width // 2
    wide = span // CHUNKS
    bf = jnp.bfloat16
    dma = pltpu.SemaphoreType.DMA
    vmem = pl.BlockSpec(memory_space=pltpu.VMEM)
    hbm = pl.BlockSpec(memory_space=pl.ANY)
    return pl.pallas_call(
        functools.partial(kernel, side),
        out_shape=jax.ShapeDtypeStruct((count, width), bf),
        in_specs=[hbm] + [vmem] * 4 + [hbm] * 3,
        out_specs=hbm,
        scratch_shapes=[
            pltpu.VMEM((count, width), bf),
            pltpu.VMEM((count, span), bf),
            pltpu.VMEM((LINE, 2, count, span), bf),
            pltpu.VMEM((LINE, 2, 8, count), jnp.float32),
            pltpu.VMEM((width, half), bf),
            pltpu.VMEM((width, half), bf),
            pltpu.VMEM((2 * half, span), bf),
            pltpu.VMEM((LINE, 2, rows, count), bf),
            pltpu.VMEM((LINE, 2, 2, count, rows), bf),
            pltpu.VMEM((LINE, 2, rows, span), bf),
            pltpu.VMEM((LINE, 2, 2, rows, span), bf),
            pltpu.VMEM((LINE, 2, 2, rows, half), bf),
            pltpu.VMEM((LINE, 2, rows, span), bf),
            pltpu.VMEM((LINE, 2, rows, span), bf),
            pltpu.VMEM((LINE - 1, 2, CHUNKS, count, wide), bf),
            pltpu.VMEM((LINE + 1, 2, CHUNKS, count, wide), bf),
            pltpu.VMEM((2, CHUNKS, count, wide), bf),
            dma,
            dma((3,)),
            dma,
            dma,
            dma((LINE, 2, CHUNKS)),
            dma((2, LINE, 2)),
            dma((LINE, 2)),
            dma((2, LINE, 2)),
            dma((2,)),
            dma((LINE, 2)),
            dma((LINE, 2)),
            dma((LINE, 2)),
            dma((LINE, 2)),
            dma((LINE, 2)),
            dma((LINE, 2)),
            dma((LINE, 2, CHUNKS)),
            dma((LINE, 2)),
            dma((LINE + 1, 2, CHUNKS)),
            dma((LINE - 1, 2)),
            dma,
            dma,
            dma,
        ],
        compiler_params=pltpu.CompilerParams(
            collective_id=0, has_side_effects=True, vmem_limit_bytes=60 * 1024 * 1024
        ),
    )(
        tokens, norm_gain[None], norm_bias[None], expert_ids.T, route_weights.T,
        gate_weight, up_weight, down_weight,
    )


def solution(mesh):
    placed = (
        P(("ep", "tp"), None),
        P(),
        P(),
        P("ep", None, "tp"),
        P("ep", None, "tp"),
        P("ep", "tp", None),
        P(("ep", "tp"), None),
        P(("ep", "tp"), None),
    )
    return jax.shard_map(
        body, mesh=mesh, in_specs=placed, out_specs=P(("ep", "tp"), None), check_vma=False
    )
```

time: 135 us -> 119 us (0.88)
  Pallas kernels: 130 us -> 115 us
  other arithmetic: 1.37 us -> 0 us
    pallas_call x1, Pallas kernels: 130 us -> 115 us  [body(): pl.pallas_call(functools.partial(kernel, side), out_shape=jax.ShapeDtypeS...]
where the time goes in v1:
time: 119 us; the launch traced here: 117 us
  Pallas kernels  115 us (97%)
  local copies, waits for them, and re-layouts  2.3 us (2%)
    pallas_call x1, Pallas kernels, body(): pl.pallas_call(functools.partial(kernel, side), out_shape=jax.ShapeDtypeS...  115 us

profile of v1, /device:TPU:0, one launch (start us, length us, event | category | flops | bytes accessed | tf_op | source)
XLA Modules:
  0.0 117.3 jit_solution(9734685700575840743)
XLA Ops:
  0.0 115.0 %shard_map.82 = bf16[256,2048]{1,0:T(8,128)(2,1)} custom-call(bf16[256,2048]{1,0:T(8,128)(2,1)} %raw.1, f32[1,2048]{1,0:T(1,128)} %bitcast.4, f32[1,2048]{1,0:T(1,128)} %bitcast.5, s32[2,256]{1,0:T(2,128)} %bitcast.6, f32[2,256]{1,0:T(2,128)} %bitcast.7, bf16[1,2048,512]{2,1,0:T(8,128)(2,1)} %gw.1, bf16[1,2048,512]{2,1,0:T(8,128)(2,1)} %uw.1, ...), custom_call_target="tpu_custom_call" | custom-call | tf_op jit(solution)/shard_map/pallas_call | solution.py:565
  115.0 2.3 %copy.10 = bf16[256,2048]{1,0:T(8,128)(2,1)} copy(bf16[256,2048]{1,0:T(8,128)(2,1)} %shard_map.82) | data formatting | bytes 2097152

commit v2 on v1

--- a/solution.py
+++ b/solution.py
@@ -13,10 +13,10 @@
 
 
 def kernel(
-    planes, raw, gain, bias, ids, rw, gw, uw, dw, out,
-    src, oth, tok, met, wg, wu, wd, sel, mix, snd, xin, hid, res, ret, psend, racc, obuf,
-    s_own, s_wl, s_ws, s_wr, s_tok, s_toks, s_met, s_mets, s_os, s_x, s_xs, s_xd, s_xds,
-    s_h, s_hs, s_r, s_rs, s_p, s_ps, s_ol, s_or, s_od,
+    planes, raw, gain_in, bias_in, ids_in, rw_in, gw, uw, dw, out,
+    src, gain, bias, ids, rw, oth, tok, met, wg, wu, wd, sel, mix, snd, xin, hid, res, ret, psend, racc, obuf,
+    s_own, s_lent, s_wl, s_ws, s_wr, s_tok, s_toks, s_met, s_mets, s_os, s_x, s_xs, s_xd, s_xds,
+    s_h, s_hs, s_r, s_rs, s_p, s_ps, s_or, s_od,
 ):
     n = LINE
     side = planes
@@ -68,8 +68,19 @@
         pltpu.make_async_copy(ref, ref, sem).wait()
 
     barrier = pltpu.get_barrier_semaphore()
-    own = pltpu.make_async_copy(raw, src, s_own)
-    own.start()
+    small = [(ids_in, ids), (rw_in, rw), (gain_in, gain), (bias_in, bias)]
+    slab = min(64, tokens)
+    turns = tokens // slab
+
+    def fetch(i):
+        at = part(i, slab)
+        return pltpu.make_async_copy(raw.at[at], src.at[at], s_own.at[len(small) + i])
+
+    fetch(0).start()
+    for i, (a, b) in enumerate(small):
+        pltpu.make_async_copy(a, b, s_own.at[i]).start()
+    for i in range(1, turns):
+        fetch(i).start()
 
     def greet(where):
         pl.semaphore_signal(barrier, inc=1, device_id=where, device_id_type=MESH)
@@ -91,15 +102,14 @@
     for i, (a, b) in enumerate(loads):
         pltpu.make_async_copy(a, b, s_wl.at[i]).start()
 
+    for i, (a, b) in enumerate(small):
+        pltpu.make_async_copy(a, b, s_own.at[i]).wait()
     met[z, core, 0:2, :] = ids[...].astype(jnp.float32)
     met[z, core, 2:4, :] = rw[...]
 
-    own.wait()
-    slab = min(32, tokens)
-
-    @pl.loop(0, tokens // slab)
-    def _(i):
-        at = pl.ds(pl.multiple_of(i * slab, slab), slab)
+    def lnorm(i):
+        fetch(i).wait()
+        at = part(i, slab)
         v = src[at, :].astype(jnp.float32)
         v = v - jnp.mean(v, axis=-1, keepdims=True)
         spread = jnp.mean(v * v, axis=-1, keepdims=True)
@@ -109,13 +119,22 @@
         tok[z, core, at, :] = jnp.where(core == 0, lo, hi)
         oth[at, :] = jnp.where(core == 0, hi, lo)
 
-    pl.semaphore_wait(barrier, side + 1 + jnp.where(mid, 1, 0))
-
+    def waitbar():
+        pl.semaphore_wait(barrier, side + 1 + jnp.where(mid, 1, 0))
+
+    block = tokens // 2
+
+    def lend(h):
+        at = part(h, block)
+        remote(oth.at[at], tok.at[z, core, at], s_os.at[1], s_lent.at[h], partner)
+
+    pl.loop(0, turns // 2)(lnorm)
+    waitbar()
     remote(met.at[z, core], met.at[z, core], s_os.at[0], s_met.at[z, core], partner)
-    for c in range(k):
-        remote(
-            oth.at[:, cols(c)], tok.at[z, core, :, cols(c)], s_os.at[1], s_tok.at[z, core, c], partner
-        )
+    lend(0)
+    pl.loop(turns // 2, turns)(lnorm)
+    lend(1)
+
     remote(
         dw.at[0, :, part(other, span)], wd.at[mine], s_ws, s_wr, partner
     )
@@ -134,17 +153,18 @@
     def got_met(s, b):
         landed(met.at[s, b], s_met.at[s, b])
 
-    def own_tok(b):
-        for c in range(k):
-            @pl.when(core != b)
-            def _():
-                arrived(z, b, c)
-
+    def lent():
+        for h in range(2):
+            landed(oth.at[part(h, block)], s_lent.at[h])
+
+    def own_tok(b, lo, hi):
+        for c in range(lo, hi):
             send_tok(z, b, c, za, 0)
 
-    def own_tok_b(b):
-        for c in range(k):
-            send_tok(z, b, c, zb, 1)
+            if b == 0:
+                @pl.when(mid)
+                def _():
+                    send_tok(z, b, c, zb, 1)
 
     def prep(q, b, s=None):
         s = order[q] if s is None else s
@@ -177,16 +197,18 @@
             o = peer(j)
             remote(
                 snd.at[q, b, band(o), cols(c)], xin.at[q, b, core, band(p), cols(c)],
-                s_xs.at[q, b], s_x.at[q, b], {"ep": z * side + o},
+                s_xs.at[q, b], s_x.at[q, b, c], {"ep": z * side + o},
             )
 
     def others(ref):
         return ref.at[pl.ds(0, (side - 1) * cap)]
 
     def swap_x(q, b):
-        landed(others(xin.at[q, b, core]), s_x.at[q, b])
-        at = xin.at[q, b, core]
-        remote(at, at, s_xds.at[q, b], s_xd.at[q, b], partner)
+        @pl.loop(0, k)
+        def _(c):
+            at = xin.at[q, b, core, :, cols(c)]
+            landed(others(at), s_x.at[q, b, c])
+            remote(at, at, s_xds.at[q, b], s_xd.at[q, b], partner)
 
     tile = min(256, half)
 
@@ -203,9 +225,8 @@
             u = u + jnp.dot(hi, wu[span:, at], preferred_element_type=jnp.float32)
             v = g / (1.0 + jnp.exp(-g)) * u
             hid[q, b, core, :, at] = v.astype(jnp.bfloat16)
-
-        at = hid.at[q, b, core]
-        remote(at, at, s_hs.at[q, b], s_h.at[q, b], partner)
+            done = hid.at[q, b, core, :, at]
+            remote(done, done, s_hs.at[q, b], s_h.at[q, b], partner)
 
     def down(q, b, c):
         @pl.when(c == 0)
@@ -257,27 +278,19 @@
             send_met(z, b, zb, 1)
 
     own_met(core)
-    own_tok(0)
-
-    @pl.when(mid)
-    def _():
-        own_tok_b(0)
-
+    pl.when(core == 1)(lent)
+    own_tok(0, 0, 1)
     got_met(z, other)
     own_met(other)
+    own_tok(0, 1, k)
     prep(0, 0)
     pl.loop(0, k)(lambda c: disp(0, 0, c))
 
+    pl.when(core == 0)(lent)
+
     @pl.when(end)
     def _():
-        own_tok(1)
-
-    @pl.when(mid)
-    def _():
-        @pl.when(core != 1)
-        def _():
-            for c in range(k):
-                arrived(z, 1, c)
+        own_tok(1, 0, k)
 
     prep(0, 1)
 
@@ -373,13 +386,9 @@
             def _():
                 gate(1, 1)
 
-            @pl.when(c > 0)
-            def _():
-                fold(3, 0, c - 1)
-
         pl.loop(0, k)(lambda c: send_tok(z, 1, c, zb, 1))
         pl.loop(0, k)(lambda c: disp(2, 1, c))
-        fold(3, 0, k - 1)
+        folds(3, 0, 0, k)
         downs(1, 1)
         folds(1, 0, 0, k // 2)
         swap_x(3, 1)
@@ -418,8 +427,6 @@
 
     @pl.when(end)
     def _():
-        pl.loop(0, k)(lambda c: disp(0, 1, c))
-
         def take(q, b, c):
             s = z + (n - q) * step
             arrived(s, b, c)
@@ -441,6 +448,7 @@
         @pl.loop(0, k)
         def _(c):
             take(3, 0, c)
+            disp(0, 1, c)
 
             @pl.when(c == 1)
             def _():
@@ -451,6 +459,7 @@
             def _():
                 gate(0, 0)
 
+        pl.loop(0, k // 2)(lambda c: down(0, 0, c))
         quarter = k // 4
 
         @pl.loop(0, 5)
@@ -477,20 +486,27 @@
             back(3)
             more(3)
             pl.loop(k // 2, k)(lambda c: down(q, b, c))
+
+            @pl.when(i == 1)
+            def _():
+                swap_x(0, 1)
+
+            @pl.when(i == 2)
+            def _():
+                gate(0, 1)
+
+            @pl.when(i == 4)
+            def _():
+                downs(0, 1)
+
             pl.loop(0, quarter)(lambda c: fold(q, b, c))
-
-            @pl.when(i == 0)
-            def _():
-                swap_x(0, 1)
-                downs(0, 0)
-                gate(0, 1)
 
         swap_x(3, 1)
         pl.loop(quarter, 2 * quarter)(lambda c: fold(2, 1, c))
         gate(3, 1)
         pl.loop(2 * quarter, k)(lambda c: fold(2, 1, c))
         downs(3, 1)
-        downs(0, 1)
+        pl.loop(k // 2, k)(lambda c: down(0, 0, c))
         pl.loop(0, k)(lambda c: fold(3, 1, c))
 
     def last(b, c, slots):
@@ -498,16 +514,16 @@
         for slot in slots:
             landed(racc.at[slot, b, c], s_p.at[slot, b, c])
             y = y + racc[slot, b, c].astype(jnp.float32)
-        obuf[b, c] = y.astype(out.dtype)
-        to = out.at[:, pl.ds(pl.multiple_of(core * span + c * wide, wide), wide)]
+        to = pl.ds(pl.multiple_of(core * span + c * wide, wide), wide)
 
         @pl.when(core == b)
         def _():
-            pltpu.make_async_copy(obuf.at[b, c], to, s_ol).start()
+            out[:, to] = y.astype(out.dtype)
 
         @pl.when(core != b)
         def _():
-            remote(obuf.at[b, c], to, s_od, s_or, partner)
+            obuf[c] = y.astype(out.dtype)
+            remote(obuf.at[c], out.at[:, to], s_od, s_or, partner)
 
     @pl.when(end)
     def _():
@@ -542,9 +558,8 @@
             drain(hid.at[q, b, core], s_hs.at[q, b])
             if q > 0:
                 drain(psend.at[q - 1, b], s_ps.at[q - 1, b])
-    drain(obuf.at[0], s_ol)
-    drain(obuf.at[0], s_od)
-    drain(obuf.at[0], s_or)
+    drain(obuf, s_od)
+    drain(obuf, s_or)
 
 
 def body(
@@ -560,15 +575,18 @@
     wide = span // CHUNKS
     bf = jnp.bfloat16
     dma = pltpu.SemaphoreType.DMA
-    vmem = pl.BlockSpec(memory_space=pltpu.VMEM)
     hbm = pl.BlockSpec(memory_space=pl.ANY)
     return pl.pallas_call(
         functools.partial(kernel, side),
-        out_shape=jax.ShapeDtypeStruct((count, width), bf),
-        in_specs=[hbm] + [vmem] * 4 + [hbm] * 3,
-        out_specs=hbm,
+        out_shape=pltpu.VMEM((count, width), bf),
+        in_specs=[hbm] * 8,
+        out_specs=pl.BlockSpec(memory_space=pltpu.VMEM),
         scratch_shapes=[
             pltpu.VMEM((count, width), bf),
+            pltpu.VMEM((1, width), jnp.float32),
+            pltpu.VMEM((1, width), jnp.float32),
+            pltpu.VMEM((2, count), jnp.int32),
+            pltpu.VMEM((2, count), jnp.float32),
             pltpu.VMEM((count, span), bf),
             pltpu.VMEM((LINE, 2, count, span), bf),
             pltpu.VMEM((LINE, 2, 8, count), jnp.float32),
@@ -584,8 +602,9 @@
             pltpu.VMEM((LINE, 2, rows, span), bf),
             pltpu.VMEM((LINE - 1, 2, CHUNKS, count, wide), bf),
             pltpu.VMEM((LINE + 1, 2, CHUNKS, count, wide), bf),
-            pltpu.VMEM((2, CHUNKS, count, wide), bf),
-            dma,
+            pltpu.VMEM((CHUNKS, count, wide), bf),
+            dma((4 + count // min(64, count),)),
+            dma((2,)),
             dma((3,)),
             dma,
             dma,
@@ -594,7 +613,7 @@
             dma((LINE, 2)),
             dma((2, LINE, 2)),
             dma((2,)),
-            dma((LINE, 2)),
+            dma((LINE, 2, CHUNKS)),
             dma((LINE, 2)),
             dma((LINE, 2)),
             dma((LINE, 2)),
@@ -606,10 +625,9 @@
             dma((LINE - 1, 2)),
             dma,
             dma,
-            dma,
         ],
         compiler_params=pltpu.CompilerParams(
-            collective_id=0, has_side_effects=True, vmem_limit_bytes=60 * 1024 * 1024
+            collective_id=0, has_side_effects=True, vmem_limit_bytes=56 * 1024 * 1024
         ),
     )(
         tokens, norm_gain[None], norm_bias[None], expert_ids.T, route_weights.T,

time: 119 us -> 108 us (0.908)
  Pallas kernels: 115 us -> 105 us
  local copies, waits for them, and re-layouts: 2.3 us -> 0.97 us
    pallas_call x1, Pallas kernels: 115 us -> 105 us  [body(): pl.pallas_call(functools.partial(kernel, side), out_shape=pltpu.VMEM((cou...]
    unnamed x1, local copies, waits for them, and re-layouts: 2.3 us -> 0.97 us
where the time goes in v2:
time: 108 us; the launch traced here: 106 us
  Pallas kernels  105 us (97%)
    pallas_call x1, Pallas kernels, body(): pl.pallas_call(functools.partial(kernel, side), out_shape=pltpu.VMEM((cou...  105 us

profile of v2, /device:TPU:0, one launch (start us, length us, event | category | flops | bytes accessed | tf_op | source)
XLA Modules:
  0.0 106.3 jit_solution(3695765564592195826)
XLA Ops:
  0.0 105.4 %shard_map.82 = bf16[256,2048]{1,0:T(8,128)(2,1)S(1)} custom-call(bf16[256,2048]{1,0:T(8,128)(2,1)} %raw.1, f32[1,2048]{1,0:T(1,128)} %bitcast.4, f32[1,2048]{1,0:T(1,128)} %bitcast.5, s32[2,256]{1,0:T(2,128)} %bitcast.6, f32[2,256]{1,0:T(2,128)} %bitcast.7, bf16[1,2048,512]{2,1,0:T(8,128)(2,1)} %gw.1, bf16[1,2048,512]{2,1,0:T(8,128)(2,1)} %uw.1, ...), custom_call_target="tpu_custom_call" | custom-call | tf_op jit(solution)/shard_map/pallas_call | solution.py:579
  105.4 1.0 copy.10

commit v3 on v2

--- a/solution.py
+++ b/solution.py
@@ -104,8 +104,11 @@
 
     for i, (a, b) in enumerate(small):
         pltpu.make_async_copy(a, b, s_own.at[i]).wait()
-    met[z, core, 0:2, :] = ids[...].astype(jnp.float32)
-    met[z, core, 2:4, :] = rw[...]
+    fold_at = tokens // 2
+    facts = [ids[0:1].astype(jnp.float32), ids[1:2].astype(jnp.float32), rw[0:1], rw[1:2]]
+    for i, fact in enumerate(facts):
+        met[z, core, 2 * i : 2 * i + 1, :] = fact[:, :fold_at]
+        met[z, core, 2 * i + 1 : 2 * i + 2, :] = fact[:, fold_at:]
 
     def lnorm(i):
         fetch(i).wait()
@@ -122,30 +125,28 @@
     def waitbar():
         pl.semaphore_wait(barrier, side + 1 + jnp.where(mid, 1, 0))
 
-    block = tokens // 2
-
     def lend(h):
-        at = part(h, block)
-        remote(oth.at[at], tok.at[z, core, at], s_os.at[1], s_lent.at[h], partner)
+        at = part(h, slab)
+        remote(oth.at[at], tok.at[z, core, at], s_os.at[1], s_lent, partner)
 
     pl.loop(0, turns // 2)(lnorm)
     waitbar()
     remote(met.at[z, core], met.at[z, core], s_os.at[0], s_met.at[z, core], partner)
-    lend(0)
-    pl.loop(turns // 2, turns)(lnorm)
-    lend(1)
-
-    remote(
-        dw.at[0, :, part(other, span)], wd.at[mine], s_ws, s_wr, partner
-    )
+    pl.loop(0, turns // 2)(lend)
+
+    @pl.loop(turns // 2, turns)
+    def _(i):
+        lnorm(i)
+        lend(i)
+
 
     def send_tok(s, b, c, to, way):
         at = tok.at[s, b, :, cols(c)]
-        remote(at, at, s_toks.at[way, s, b], s_tok.at[s, b, c], plane(to))
+        remote(at, at, s_toks.at[way], s_tok.at[s, b, c], plane(to))
 
     def send_met(s, b, to, way):
         at = met.at[s, b]
-        remote(at, at, s_mets.at[way, s, b], s_met.at[s, b], plane(to))
+        remote(at, at, s_mets.at[way], s_met.at[s, b], plane(to))
 
     def arrived(s, b, c):
         landed(tok.at[s, b, :, cols(c)], s_tok.at[s, b, c])
@@ -154,8 +155,7 @@
         landed(met.at[s, b], s_met.at[s, b])
 
     def lent():
-        for h in range(2):
-            landed(oth.at[part(h, block)], s_lent.at[h])
+        landed(oth, s_lent)
 
     def own_tok(b, lo, hi):
         for c in range(lo, hi):
@@ -168,8 +168,10 @@
 
     def prep(q, b, s=None):
         s = order[q] if s is None else s
-        ids0, ids1 = met[s, b, 0:1, :], met[s, b, 1:2, :]
-        wt0, wt1 = met[s, b, 2:3, :], met[s, b, 3:4, :]
+        ids0, ids1, wt0, wt1 = [
+            jnp.concatenate([met[s, b, 2 * i : 2 * i + 1], met[s, b, 2 * i + 1 : 2 * i + 2]], axis=1)
+            for i in range(4)
+        ]
         row = lax.broadcasted_iota(jnp.int32, (rows, tokens), 0)
         e_row = (z * side + row // cap).astype(jnp.float32)
         s_row = lax.rem(row, cap).astype(jnp.float32)
@@ -197,7 +199,7 @@
             o = peer(j)
             remote(
                 snd.at[q, b, band(o), cols(c)], xin.at[q, b, core, band(p), cols(c)],
-                s_xs.at[q, b], s_x.at[q, b, c], {"ep": z * side + o},
+                s_xs, s_x.at[q, b, c], {"ep": z * side + o},
             )
 
     def others(ref):
@@ -208,7 +210,7 @@
         def _(c):
             at = xin.at[q, b, core, :, cols(c)]
             landed(others(at), s_x.at[q, b, c])
-            remote(at, at, s_xds.at[q, b], s_xd.at[q, b], partner)
+            remote(at, at, s_xds, s_xd.at[q, b], partner)
 
     tile = min(256, half)
 
@@ -226,7 +228,7 @@
             v = g / (1.0 + jnp.exp(-g)) * u
             hid[q, b, core, :, at] = v.astype(jnp.bfloat16)
             done = hid.at[q, b, core, :, at]
-            remote(done, done, s_hs.at[q, b], s_h.at[q, b], partner)
+            remote(done, done, s_hs, s_h.at[q, b], partner)
 
     def down(q, b, c):
         @pl.when(c == 0)
@@ -241,7 +243,7 @@
             o = peer(j)
             remote(
                 res.at[q, b, band(o), cols(c)], ret.at[q, b, band(p), cols(c)],
-                s_rs.at[q, b], s_r.at[q, b, c], {"ep": z * side + o},
+                s_rs, s_r.at[q, b, c], {"ep": z * side + o},
             )
 
     def downs(q, b):
@@ -262,7 +264,7 @@
         psend[q - 1, b, c] = y.astype(jnp.bfloat16)
         slot = jnp.where((to == t) & (to < z), n, t)
         remote(
-            psend.at[q - 1, b, c], racc.at[slot, b, c], s_ps.at[q - 1, b], s_p.at[slot, b, c], plane(to)
+            psend.at[q - 1, b, c], racc.at[slot, b, c], s_ps, s_p.at[slot, b, c], plane(to)
         )
 
     def weights():
@@ -277,22 +279,31 @@
         def _():
             send_met(z, b, zb, 1)
 
-    own_met(core)
-    pl.when(core == 1)(lent)
-    own_tok(0, 0, 1)
-    got_met(z, other)
-    own_met(other)
-    own_tok(0, 1, k)
+    @pl.when(core == 0)
+    def _():
+        own_met(0)
+        own_tok(0, 0, k)
+
+    @pl.when(core == 1)
+    def _():
+        prep(0, 1)
+        got_met(z, 0)
+        own_met(0)
+        lent()
+        own_tok(0, 0, k)
+
     prep(0, 0)
     pl.loop(0, k)(lambda c: disp(0, 0, c))
-
-    pl.when(core == 0)(lent)
-
-    @pl.when(end)
-    def _():
-        own_tok(1, 0, k)
-
-    prep(0, 1)
+    remote(dw.at[0, :, part(other, span)], wd.at[mine], s_ws, s_wr, partner)
+
+    @pl.when(core == 0)
+    def _():
+        got_met(z, 1)
+        lent()
+        prep(0, 1)
+
+    own_met(1)
+    pl.when(end)(lambda: own_tok(1, 0, k))
 
     @pl.when(mid)
     def _():
@@ -448,7 +459,10 @@
         @pl.loop(0, k)
         def _(c):
             take(3, 0, c)
-            disp(0, 1, c)
+
+            @pl.when(c < k // 2)
+            def _():
+                disp(0, 1, c)
 
             @pl.when(c == 1)
             def _():
@@ -459,33 +473,41 @@
             def _():
                 gate(0, 0)
 
-        pl.loop(0, k // 2)(lambda c: down(0, 0, c))
         quarter = k // 4
 
-        @pl.loop(0, 5)
+        def piece(f, q, b, j, m=1):
+            pl.loop(j * quarter, (j + m) * quarter)(lambda c: f(q, b, c))
+
+        piece(disp, 0, 1, 2, 2)
+        piece(down, 0, 0, 0)
+        learn(2, 0)
+        swap_x(3, 0)
+        piece(take, 2, 0, 0)
+        gate(3, 0)
+        piece(take, 2, 0, 1)
+        piece(down, 3, 0, 0, 2)
+        piece(take, 2, 0, 2)
+        piece(take, 2, 0, 3)
+        piece(down, 3, 0, 2, 2)
+        piece(fold, 3, 0, 0)
+
+        @pl.loop(1, 5)
         def _(i):
             q, b = unit(i)
             q1, b1 = unit(i + 1)
-            q0, b0 = unit(jnp.maximum(i - 1, 0))
-
-            def more(j):
-                pl.loop(j * quarter, (j + 1) * quarter)(lambda c: take(q1, b1, c))
-
-            def back(j):
-                pl.when(i > 0)(lambda: pl.loop(j * quarter, (j + 1) * quarter)(lambda c: fold(q0, b0, c)))
-
+            q0, b0 = unit(i - 1)
             learn(q1, b1)
-            more(0)
+            piece(take, q1, b1, 0)
+            piece(fold, q0, b0, 1)
             swap_x(q, b)
-            back(1)
-            more(1)
+            piece(take, q1, b1, 1)
             gate(q, b)
-            back(2)
-            more(2)
-            pl.loop(0, k // 2)(lambda c: down(q, b, c))
-            back(3)
-            more(3)
-            pl.loop(k // 2, k)(lambda c: down(q, b, c))
+            piece(fold, q0, b0, 2)
+            piece(take, q1, b1, 2)
+            piece(down, q, b, 0, 2)
+            piece(fold, q0, b0, 3)
+            piece(take, q1, b1, 3)
+            piece(down, q, b, 2, 2)
 
             @pl.when(i == 1)
             def _():
@@ -497,17 +519,18 @@
 
             @pl.when(i == 4)
             def _():
-                downs(0, 1)
-
-            pl.loop(0, quarter)(lambda c: fold(q, b, c))
+                piece(down, 0, 1, 0, 3)
+
+            piece(fold, q, b, 0)
 
         swap_x(3, 1)
-        pl.loop(quarter, 2 * quarter)(lambda c: fold(2, 1, c))
+        piece(fold, 2, 1, 1)
         gate(3, 1)
-        pl.loop(2 * quarter, k)(lambda c: fold(2, 1, c))
+        piece(fold, 2, 1, 2, 2)
         downs(3, 1)
-        pl.loop(k // 2, k)(lambda c: down(0, 0, c))
-        pl.loop(0, k)(lambda c: fold(3, 1, c))
+        piece(down, 0, 0, 1, 3)
+        piece(down, 0, 1, 3)
+        piece(fold, 3, 1, 0, 4)
 
     def last(b, c, slots):
         y = weigh(0, b, c)
@@ -539,25 +562,24 @@
     drain(met.at[z, core], s_os.at[0])
     drain(oth, s_os.at[1])
     drain(wd.at[mine], s_ws)
-    for b in range(2):
-        drain(tok.at[z, b], s_toks.at[0, z, b])
-        drain(met.at[z, b], s_mets.at[0, z, b])
+    sent = pl.ds(0, (side - 1) * cap)
+
+    @pl.when(end)
+    def _():
+        drain(tok.at[0], s_toks.at[0])
+        drain(met.at[0], s_mets.at[0])
 
     @pl.when(mid)
     def _():
-        for b in range(2):
-            for way, s in ((1, z), (0, order[2]), (1, order[1]), (1, order[3])):
-                drain(tok.at[s, b], s_toks.at[way, s, b])
-                drain(met.at[s, b], s_mets.at[way, s, b])
-
-    for q in range(n):
-        for b in range(2):
-            drain(others(snd.at[q, b]), s_xs.at[q, b])
-            drain(others(res.at[q, b]), s_rs.at[q, b])
-            drain(xin.at[q, b, core], s_xds.at[q, b])
-            drain(hid.at[q, b, core], s_hs.at[q, b])
-            if q > 0:
-                drain(psend.at[q - 1, b], s_ps.at[q - 1, b])
+        for way in range(2):
+            drain(tok.at[pl.ds(0, 2 + way)], s_toks.at[way])
+            drain(met.at[pl.ds(0, 2 + way)], s_mets.at[way])
+
+    drain(snd.at[:, :, sent], s_xs)
+    drain(res.at[:, :, sent], s_rs)
+    drain(snd, s_xds)
+    drain(hid.at[:, :, 0], s_hs)
+    drain(psend, s_ps)
     drain(obuf, s_od)
     drain(obuf, s_or)
 
@@ -589,7 +611,7 @@
             pltpu.VMEM((2, count), jnp.float32),
             pltpu.VMEM((count, span), bf),
             pltpu.VMEM((LINE, 2, count, span), bf),
-            pltpu.VMEM((LINE, 2, 8, count), jnp.float32),
+            pltpu.VMEM((LINE, 2, 8, count // 2), jnp.float32),
             pltpu.VMEM((width, half), bf),
             pltpu.VMEM((width, half), bf),
             pltpu.VMEM((2 * half, span), bf),
@@ -604,25 +626,25 @@
             pltpu.VMEM((LINE + 1, 2, CHUNKS, count, wide), bf),
             pltpu.VMEM((CHUNKS, count, wide), bf),
             dma((4 + count // min(64, count),)),
+            dma,
+            dma((3,)),
+            dma,
+            dma,
+            dma((LINE, 2, CHUNKS)),
             dma((2,)),
-            dma((3,)),
-            dma,
-            dma,
-            dma((LINE, 2, CHUNKS)),
-            dma((2, LINE, 2)),
             dma((LINE, 2)),
-            dma((2, LINE, 2)),
+            dma((2,)),
             dma((2,)),
             dma((LINE, 2, CHUNKS)),
+            dma,
             dma((LINE, 2)),
+            dma,
             dma((LINE, 2)),
-            dma((LINE, 2)),
-            dma((LINE, 2)),
-            dma((LINE, 2)),
+            dma,
             dma((LINE, 2, CHUNKS)),
-            dma((LINE, 2)),
+            dma,
             dma((LINE + 1, 2, CHUNKS)),
-            dma((LINE - 1, 2)),
+            dma,
             dma,
             dma,
         ],

time: 108 us -> 105 us (0.972)
  Pallas kernels: 105 us -> 103 us
    pallas_call x1, Pallas kernels: 105 us -> 103 us  [body(): pl.pallas_call(functools.partial(kernel, side), out_shape=pltpu.VMEM((cou...]
where the time goes in v3:
time: 105 us; the launch traced here: 104 us
  Pallas kernels  103 us (98%)
    pallas_call x1, Pallas kernels, body(): pl.pallas_call(functools.partial(kernel, side), out_shape=pltpu.VMEM((cou...  103 us

profile of v3, /device:TPU:0, one launch (start us, length us, event | category | flops | bytes accessed | tf_op | source)
XLA Modules:
  0.0 104.3 jit_solution(16321121088148344474)
XLA Ops:
  0.0 103.3 %shard_map.82 = bf16[256,2048]{1,0:T(8,128)(2,1)S(1)} custom-call(bf16[256,2048]{1,0:T(8,128)(2,1)} %raw.1, f32[1,2048]{1,0:T(1,128)} %bitcast.4, f32[1,2048]{1,0:T(1,128)} %bitcast.5, s32[2,256]{1,0:T(2,128)} %bitcast.6, f32[2,256]{1,0:T(2,128)} %bitcast.7, bf16[1,2048,512]{2,1,0:T(8,128)(2,1)} %gw.1, bf16[1,2048,512]{2,1,0:T(8,128)(2,1)} %uw.1, ...), custom_call_target="tpu_custom_call" | custom-call | tf_op jit(solution)/shard_map/pallas_call | solution.py:601
  103.3 1.0 copy.10

commit v4 on v3

--- a/solution.py
+++ b/solution.py
@@ -14,9 +14,9 @@
 
 def kernel(
     planes, raw, gain_in, bias_in, ids_in, rw_in, gw, uw, dw, out,
-    src, gain, bias, ids, rw, oth, tok, met, wg, wu, wd, sel, mix, snd, xin, hid, res, ret, psend, racc, obuf,
+    src, gain, bias, ids, rw, oth, tok, met, wg, wu, wd, sel, mix, snd, xin, hid, res, ret, psend, racc, home,
     s_own, s_lent, s_wl, s_ws, s_wr, s_tok, s_toks, s_met, s_mets, s_os, s_x, s_xs, s_xd, s_xds,
-    s_h, s_hs, s_r, s_rs, s_p, s_ps, s_or, s_od,
+    s_h, s_hs, s_r, s_rs, s_p, s_ps, s_home, s_rd,
 ):
     n = LINE
     side = planes
@@ -85,16 +85,17 @@
     def greet(where):
         pl.semaphore_signal(barrier, inc=1, device_id=where, device_id_type=MESH)
 
+    for twin in range(2):
+        greet({"ep": za * side + p, "tp": twin})
+
+        @pl.when(mid)
+        def _():
+            greet({"ep": zb * side + p, "tp": twin})
+
+        for j in range(1, side):
+            greet({"ep": z * side + peer(j), "tp": twin})
+
     greet(partner)
-    greet(plane(za))
-
-    @pl.when(mid)
-    def _():
-        greet(plane(zb))
-
-    for j in range(1, side):
-        greet({"ep": z * side + peer(j)})
-
     mine = part(core, half)
     loads = [
         (gw.at[0], wg), (uw.at[0], wu), (dw.at[0, :, part(core, span)], wd.at[mine]),
@@ -123,7 +124,7 @@
         oth[at, :] = jnp.where(core == 0, hi, lo)
 
     def waitbar():
-        pl.semaphore_wait(barrier, side + 1 + jnp.where(mid, 1, 0))
+        pl.semaphore_wait(barrier, 2 * side + 1 + jnp.where(mid, 2, 0))
 
     def lend(h):
         at = part(h, slab)
@@ -140,16 +141,16 @@
         lend(i)
 
 
-    def send_tok(s, b, c, to, way):
+    def send_tok(s, b, c, to, way, place):
         at = tok.at[s, b, :, cols(c)]
-        remote(at, at, s_toks.at[way], s_tok.at[s, b, c], plane(to))
+        remote(at, at, s_toks.at[way], s_tok.at[place - 1, b, c], plane(to))
 
     def send_met(s, b, to, way):
         at = met.at[s, b]
         remote(at, at, s_mets.at[way], s_met.at[s, b], plane(to))
 
-    def arrived(s, b, c):
-        landed(tok.at[s, b, :, cols(c)], s_tok.at[s, b, c])
+    def arrived(q, s, b, c):
+        landed(tok.at[s, b, :, cols(c)], s_tok.at[q - 1, b, c])
 
     def got_met(s, b):
         landed(met.at[s, b], s_met.at[s, b])
@@ -159,12 +160,12 @@
 
     def own_tok(b, lo, hi):
         for c in range(lo, hi):
-            send_tok(z, b, c, za, 0)
+            send_tok(z, b, c, za, 0, jnp.where(end, 2, 3))
 
             if b == 0:
                 @pl.when(mid)
                 def _():
-                    send_tok(z, b, c, zb, 1)
+                    send_tok(z, b, c, zb, 1, 3)
 
     def prep(q, b, s=None):
         s = order[q] if s is None else s
@@ -238,34 +239,57 @@
         y = jnp.dot(hid[q, b, 0], wd[:half, cols(c)], preferred_element_type=jnp.float32)
         y = y + jnp.dot(hid[q, b, 1], wd[half:, cols(c)], preferred_element_type=jnp.float32)
         res[q, b, :, cols(c)] = y.astype(jnp.bfloat16)
-        ret[q, b, band(p), cols(c)] = res[q, b, band(p), cols(c)]
+        yours = isinstance(q, int) and q == 0
+        slot = core if yours else b
+        at = ret.at[q, slot, band(p), cols(c)]
+
+        def keep():
+            ret[q, slot, band(p), cols(c)] = res[q, b, band(p), cols(c)]
+
+        if yours:
+            pl.when(core == b)(keep)
+
+            @pl.when(core != b)
+            def _():
+                remote(res.at[q, b, band(p), cols(c)], at, s_rd, s_r.at[q, slot, c], partner)
+        else:
+            keep()
         for j in range(1, side):
             o = peer(j)
-            remote(
-                res.at[q, b, band(o), cols(c)], ret.at[q, b, band(p), cols(c)],
-                s_rs, s_r.at[q, b, c], {"ep": z * side + o},
-            )
+            where = {"ep": z * side + o, "tp": b} if yours else {"ep": z * side + o}
+            remote(res.at[q, b, band(o), cols(c)], at, s_rs, s_r.at[q, slot, c], where)
 
     def downs(q, b):
         pl.loop(0, k)(lambda c: down(q, b, c))
 
-    def weigh(q, b, c):
-        landed(others(ret.at[q, b, :, cols(c)]), s_r.at[q, b, c])
-        r = ret[q, b, :, cols(c)]
+    def mixed(q, b, r):
         return jnp.dot(mix[q, b, 0], r, preferred_element_type=jnp.float32) + jnp.dot(
             mix[q, b, 1], r, preferred_element_type=jnp.float32
         )
 
     def combine(q, b, c, t, to, add):
-        y = weigh(q, b, c)
+        landed(others(ret.at[q, b, :, cols(c)]), s_r.at[q, b, c])
+        y = mixed(q, b, ret[q, b, :, cols(c)])
         if add:
-            landed(racc.at[t, b, c], s_p.at[t, b, c])
-            y = y + racc[t, b, c].astype(jnp.float32)
+            landed(racc.at[q - 1, b, c], s_p.at[q - 1, b, c])
+            y = y + racc[q - 1, b, c].astype(jnp.float32)
         psend[q - 1, b, c] = y.astype(jnp.bfloat16)
-        slot = jnp.where((to == t) & (to < z), n, t)
-        remote(
-            psend.at[q - 1, b, c], racc.at[slot, b, c], s_ps, s_p.at[slot, b, c], plane(to)
-        )
+        theirs = to == t
+
+        @pl.when(theirs)
+        def _():
+            way = jnp.where(end, 1, 0)
+            remote(
+                psend.at[q - 1, b, c], home.at[way, core, c], s_ps, s_home.at[way, core, c],
+                {"ep": to * side + p, "tp": b},
+            )
+
+        @pl.when(jnp.logical_not(theirs))
+        def _():
+            slot = jnp.where(end, jnp.where(q == 1, 0, 2), 1)
+            remote(
+                psend.at[q - 1, b, c], racc.at[slot, b, c], s_ps, s_p.at[slot, b, c], plane(to)
+            )
 
     def weights():
         for i, (a, b) in enumerate(loads):
@@ -287,6 +311,7 @@
     @pl.when(core == 1)
     def _():
         prep(0, 1)
+        disp(0, 1, 0)
         got_met(z, 0)
         own_met(0)
         lent()
@@ -303,14 +328,19 @@
         prep(0, 1)
 
     own_met(1)
+    def spare(c):
+        @pl.when((core == 0) | (c > 0))
+        def _():
+            disp(0, 1, c)
+
     pl.when(end)(lambda: own_tok(1, 0, k))
 
     @pl.when(mid)
     def _():
         def relay(q, b, c):
             s = order[q]
-            arrived(s, b, c)
-            send_tok(s, b, c, za if q == 2 else zb, 0 if q == 2 else 1)
+            arrived(q, s, b, c)
+            send_tok(s, b, c, za if q == 2 else zb, 0 if q == 2 else 1, 2 if q == 3 else 1)
 
         def learn(q, b):
             got_met(order[q], b)
@@ -331,7 +361,7 @@
             relay(3, 0, c)
             relay(2, 0, c)
             disp(3, 0, c)
-            disp(0, 1, c)
+            spare(c)
 
         learn(1, 0)
         learn(2, 1)
@@ -357,7 +387,7 @@
             def _():
                 gate(3, 0)
 
-        pl.loop(0, k)(lambda c: send_tok(z, 1, c, za, 0))
+        pl.loop(0, k)(lambda c: send_tok(z, 1, c, za, 0, 3))
         learn(1, 1)
 
         @pl.loop(0, k)
@@ -397,7 +427,7 @@
             def _():
                 gate(1, 1)
 
-        pl.loop(0, k)(lambda c: send_tok(z, 1, c, zb, 1))
+        pl.loop(0, k)(lambda c: send_tok(z, 1, c, zb, 1, 3))
         pl.loop(0, k)(lambda c: disp(2, 1, c))
         folds(3, 0, 0, k)
         downs(1, 1)
@@ -440,7 +470,7 @@
     def _():
         def take(q, b, c):
             s = z + (n - q) * step
-            arrived(s, b, c)
+            arrived(q, s, b, c)
             disp(q, b, c, s)
 
         def learn(q, b):
@@ -462,7 +492,7 @@
 
             @pl.when(c < k // 2)
             def _():
-                disp(0, 1, c)
+                spare(c)
 
             @pl.when(c == 1)
             def _():
@@ -479,7 +509,6 @@
             pl.loop(j * quarter, (j + m) * quarter)(lambda c: f(q, b, c))
 
         piece(disp, 0, 1, 2, 2)
-        piece(down, 0, 0, 0)
         learn(2, 0)
         swap_x(3, 0)
         piece(take, 2, 0, 0)
@@ -528,35 +557,33 @@
         gate(3, 1)
         piece(fold, 2, 1, 2, 2)
         downs(3, 1)
-        piece(down, 0, 0, 1, 3)
+        downs(0, 0)
         piece(down, 0, 1, 3)
         piece(fold, 3, 1, 0, 4)
 
-    def last(b, c, slots):
-        y = weigh(0, b, c)
-        for slot in slots:
-            landed(racc.at[slot, b, c], s_p.at[slot, b, c])
-            y = y + racc[slot, b, c].astype(jnp.float32)
-        to = pl.ds(pl.multiple_of(core * span + c * wide, wide), wide)
-
-        @pl.when(core == b)
-        def _():
-            out[:, to] = y.astype(out.dtype)
-
-        @pl.when(core != b)
-        def _():
-            obuf[c] = y.astype(out.dtype)
-            remote(obuf.at[c], out.at[:, to], s_od, s_or, partner)
+    def last(h, c, ways):
+        at = ret.at[0, h, :, cols(c)]
+        pl.when(core == h)(lambda: landed(others(at), s_r.at[0, h, c]))
+        pl.when(core != h)(lambda: landed(at, s_r.at[0, h, c]))
+        y = mixed(0, core, at[...])
+        for way in ways:
+            landed(home.at[way, h, c], s_home.at[way, h, c])
+            y = y + home[way, h, c].astype(jnp.float32)
+        out[:, pl.ds(pl.multiple_of(h * span + c * wide, wide), wide)] = y.astype(out.dtype)
 
     @pl.when(end)
     def _():
-        for b in range(2):
-            pl.loop(0, k)(lambda c: last(b, c, [jnp.where(z == 0, n, z)]))
+        @pl.loop(0, k)
+        def _(c):
+            last(0, c, [0])
+            last(1, c, [0])
 
     @pl.when(mid)
     def _():
-        for b in range(2):
-            pl.loop(0, k)(lambda c: last(b, c, [z, n]))
+        @pl.loop(0, k)
+        def _(c):
+            last(0, c, [0, 1])
+            last(1, c, [0, 1])
 
     drain = landed
     drain(met.at[z, core], s_os.at[0])
@@ -580,8 +607,7 @@
     drain(snd, s_xds)
     drain(hid.at[:, :, 0], s_hs)
     drain(psend, s_ps)
-    drain(obuf, s_od)
-    drain(obuf, s_or)
+    drain(res.at[0, 0, pl.ds(0, cap)], s_rd)
 
 
 def body(
@@ -623,14 +649,14 @@
             pltpu.VMEM((LINE, 2, rows, span), bf),
             pltpu.VMEM((LINE, 2, rows, span), bf),
             pltpu.VMEM((LINE - 1, 2, CHUNKS, count, wide), bf),
-            pltpu.VMEM((LINE + 1, 2, CHUNKS, count, wide), bf),
-            pltpu.VMEM((CHUNKS, count, wide), bf),
+            pltpu.VMEM((LINE - 1, 2, CHUNKS, count, wide), bf),
+            pltpu.VMEM((2, 2, CHUNKS, count, wide), bf),
             dma((4 + count // min(64, count),)),
             dma,
             dma((3,)),
             dma,
             dma,
-            dma((LINE, 2, CHUNKS)),
+            dma((LINE - 1, 2, CHUNKS)),
             dma((2,)),
             dma((LINE, 2)),
             dma((2,)),
@@ -643,9 +669,9 @@
             dma,
             dma((LINE, 2, CHUNKS)),
             dma,
-            dma((LINE + 1, 2, CHUNKS)),
-            dma,
-            dma,
+            dma((LINE - 1, 2, CHUNKS)),
+            dma,
+            dma((2, 2, CHUNKS)),
             dma,
         ],
         compiler_params=pltpu.CompilerParams(

time: 105 us -> 104 us (level)
  no operation moved by 1% of the time
where the time goes in v4:
time: 104 us
  Pallas kernels  103 us (99%)
    pallas_call x1, Pallas kernels, body(): pl.pallas_call(functools.partial(kernel, side), out_shape=pltpu.VMEM((cou...  103 us

profile of v4, /device:TPU:0, one launch (start us, length us, event | category | flops | bytes accessed | tf_op | source)
XLA Modules:
  0.0 104.2 jit_solution(13001745406549064772)
XLA Ops:
  0.0 103.2 %shard_map.82 = bf16[256,2048]{1,0:T(8,128)(2,1)S(1)} custom-call(bf16[256,2048]{1,0:T(8,128)(2,1)} %raw.1, f32[1,2048]{1,0:T(1,128)} %bitcast.4, f32[1,2048]{1,0:T(1,128)} %bitcast.5, s32[2,256]{1,0:T(2,128)} %bitcast.6, f32[2,256]{1,0:T(2,128)} %bitcast.7, bf16[1,2048,512]{2,1,0:T(8,128)(2,1)} %gw.1, bf16[1,2048,512]{2,1,0:T(8,128)(2,1)} %uw.1, ...), custom_call_target="tpu_custom_call" | custom-call | tf_op jit(solution)/shard_map/pallas_call | solution.py:627
  103.2 1.0 copy.10

commit v5 on v4

--- a/solution.py
+++ b/solution.py
@@ -128,7 +128,7 @@
 
     def lend(h):
         at = part(h, slab)
-        remote(oth.at[at], tok.at[z, core, at], s_os.at[1], s_lent, partner)
+        remote(oth.at[at], tok.at[z, core, at], s_os.at[1], s_lent.at[h // (turns // 2)], partner)
 
     pl.loop(0, turns // 2)(lnorm)
     waitbar()
@@ -156,7 +156,12 @@
         landed(met.at[s, b], s_met.at[s, b])
 
     def lent():
-        landed(oth, s_lent)
+        for h in range(2):
+            landed(oth.at[part(h, tokens // 2)], s_lent.at[h])
+
+    def send_part(at, c, to, way, place):
+        piece_at = tok.at[z, 0, at, cols(c)]
+        remote(piece_at, piece_at, s_toks.at[way], s_tok.at[place - 1, 0, c], plane(to))
 
     def own_tok(b, lo, hi):
         for c in range(lo, hi):
@@ -314,8 +319,18 @@
         disp(0, 1, 0)
         got_met(z, 0)
         own_met(0)
-        lent()
-        own_tok(0, 0, k)
+
+        for h in range(2):
+            at = part(h, tokens // 2)
+            landed(oth.at[at], s_lent.at[h])
+            for c in range(1):
+                send_part(at, c, za, 0, jnp.where(end, 2, 3))
+
+                @pl.when(mid)
+                def _():
+                    send_part(at, c, zb, 1, 3)
+
+        own_tok(0, 1, k)
 
     prep(0, 0)
     pl.loop(0, k)(lambda c: disp(0, 0, c))
@@ -652,7 +667,7 @@
             pltpu.VMEM((LINE - 1, 2, CHUNKS, count, wide), bf),
             pltpu.VMEM((2, 2, CHUNKS, count, wide), bf),
             dma((4 + count // min(64, count),)),
-            dma,
+            dma((2,)),
             dma((3,)),
             dma,
             dma,

time: 104 us -> 104 us (level)
  no operation moved by 1% of the time
where the time goes in v5:
time: 104 us
  Pallas kernels  103 us (99%)
    pallas_call x1, Pallas kernels, body(): pl.pallas_call(functools.partial(kernel, side), out_shape=pltpu.VMEM((cou...  103 us

profile of v5, /device:TPU:0, one launch (start us, length us, event | category | flops | bytes accessed | tf_op | source)
XLA Modules:
  0.0 103.8 jit_solution(2417320787426926548)
XLA Ops:
  0.0 102.9 %shard_map.82 = bf16[256,2048]{1,0:T(8,128)(2,1)S(1)} custom-call(bf16[256,2048]{1,0:T(8,128)(2,1)} %raw.1, f32[1,2048]{1,0:T(1,128)} %bitcast.4, f32[1,2048]{1,0:T(1,128)} %bitcast.5, s32[2,256]{1,0:T(2,128)} %bitcast.6, f32[2,256]{1,0:T(2,128)} %bitcast.7, bf16[1,2048,512]{2,1,0:T(8,128)(2,1)} %gw.1, bf16[1,2048,512]{2,1,0:T(8,128)(2,1)} %uw.1, ...), custom_call_target="tpu_custom_call" | custom-call | tf_op jit(solution)/shard_map/pallas_call | solution.py:642
  102.9 1.0 copy.10
